TPU v7x, 32 devices: a whole 2x2x4 slice. The times are simulated.
32 devices in a mesh: fs: 8 (over z, x), tp: 4 (over y, core).
Axes of the slice: x: 2, y: 2, z: 4, core: 2. Of those that a mesh axis runs over, the one named last changes fastest.
Arguments:
- saved_input: bfloat16 [2048, 4096], P('fs'), may hold values from -8 to 8
- query_cotangent: bfloat16 [2048, 2048], P('fs', 'tp'), may hold values from -6 to 6
- layer_cotangent: bfloat16 [2048, 4096], P('fs'), may hold values from -8 to 8
- mixed_heads: bfloat16 [2048, 2048], P('fs', 'tp'), may hold values from -6 to 6
- query_basis: bfloat16 [4096, 256], P('fs'), may hold values from -0.125 to 0.125
- output_basis: bfloat16 [4096, 256], P('fs'), may hold values from -0.125 to 0.125
- query_master: float32 [4096, 2048], P('fs', 'tp'), may hold values from -3 to 3
- output_master: float32 [4096, 2048], P('fs', 'tp'), may hold values from -3 to 3
- query_first: float32 [256, 2048], P('fs', 'tp'), may hold values from -6 to 6
- query_second: float32 [256, 2048], P('fs', 'tp'), may hold values from 0.25 to 4
- output_first: float32 [256, 2048], P('fs', 'tp'), may hold values from -6 to 6
- output_second: float32 [256, 2048], P('fs', 'tp'), may hold values from 0.25 to 4
Outputs:
- query_weight: float32 [4096, 2048], P('fs', 'tp')
- output_weight: float32 [4096, 2048], P('fs', 'tp')
- query_step: float32 [4096, 2048], P('fs', 'tp')
- output_step: float32 [4096, 2048], P('fs', 'tp')
- query_first_new: float32 [256, 2048], P('fs', 'tp')
- query_second_new: float32 [256, 2048], P('fs', 'tp')
- output_first_new: float32 [256, 2048], P('fs', 'tp')
- output_second_new: float32 [256, 2048], P('fs', 'tp')
- query_copy: bfloat16 [4096, 2048], P(None, 'tp')
- output_copy: bfloat16 [4096, 2048], P(None, 'tp')
All inputs are finite; a program needn't handle non-finite values.
Results may differ from a plain program's by a relative error of at most 0.0028.
Values may be sent and summed in bfloat16 or wider, within the bound.
A program may use at most 64 MiB of HBM per device.

v0:
```python
import jax
import jax.numpy as jnp
from jax import lax
from jax.sharding import PartitionSpec as P

QW = 2048
RANK = 256
beta_one = 0.8
beta_two = 0.9
rate = 0.1


def moment_update(low, factor, first, second):
    scaled = low * factor
    first_new = beta_one * first + (1.0 - beta_one) * scaled
    second_new = beta_two * second + (1.0 - beta_two) * scaled * scaled
    direction = (first_new / jnp.sqrt(second_new)).astype(jnp.bfloat16)
    return (first_new, second_new, direction)


def contract_tokens(left, right):
    return lax.dot_general(
        left,
        right,
        (((0,), (0,)), ((), ())),
        precision=lax.Precision.HIGHEST,
        preferred_element_type=jnp.float32,
    )


def per_device(
    saved_input,
    query_cotangent,
    layer_cotangent,
    mixed_heads,
    query_basis,
    output_basis,
    query_master,
    output_master,
    query_first,
    query_second,
    output_first,
    output_second,
):
    query_coords = jnp.dot(
        saved_input,
        lax.all_gather(query_basis, "fs", axis=0, tiled=True),
        preferred_element_type=jnp.float32,
    )
    output_coords = jnp.dot(
        layer_cotangent,
        lax.all_gather(output_basis, "fs", axis=0, tiled=True),
        preferred_element_type=jnp.float32,
    )
    query_part = contract_tokens(query_coords, query_cotangent.astype(jnp.float32))
    output_part = contract_tokens(output_coords, mixed_heads.astype(jnp.float32))
    query_low, output_low = (
        lax.psum_scatter(query_part, "fs", scatter_dimension=0, tiled=True),
        lax.psum_scatter(output_part, "fs", scatter_dimension=0, tiled=True),
    )
    local_squares = jnp.sum(query_low * query_low) + jnp.sum(output_low * output_low)
    total_squares = lax.psum(local_squares, ("fs", "tp"))
    factor = 1.0 / jnp.sqrt(1.0 + total_squares / (2.0 * RANK * QW))
    qf, qs, qdir = moment_update(query_low, factor, query_first, query_second)
    of, osec, odir = moment_update(output_low, factor, output_first, output_second)
    query_whole, output_whole = (
        lax.all_gather(qdir, "fs", axis=0, tiled=True),
        lax.all_gather(odir, "fs", axis=0, tiled=True),
    )
    query_step = jnp.dot(query_basis, query_whole, preferred_element_type=jnp.float32)
    output_step = jnp.dot(output_basis, output_whole, preferred_element_type=jnp.float32)
    query_weight = query_master - rate * query_step
    output_weight = output_master - rate * output_step
    query_copy, output_copy = (
        lax.all_gather(query_weight.astype(jnp.bfloat16), "fs", axis=0, tiled=True),
        lax.all_gather(output_weight.astype(jnp.bfloat16), "fs", axis=0, tiled=True),
    )
    return (
        query_weight,
        output_weight,
        query_step,
        output_step,
        qf,
        qs,
        of,
        osec,
        query_copy,
        output_copy,
    )


def solution(mesh):
    placed = (
        P("fs", None),
        P("fs", "tp"),
        P("fs", None),
        P("fs", "tp"),
        P("fs", None),
        P("fs", None),
        P("fs", "tp"),
        P("fs", "tp"),
        P("fs", "tp"),
        P("fs", "tp"),
        P("fs", "tp"),
        P("fs", "tp"),
    )
    return jax.shard_map(
        per_device,
        mesh=mesh,
        in_specs=placed,
        out_specs=(
            P("fs", "tp"),
            P("fs", "tp"),
            P("fs", "tp"),
            P("fs", "tp"),
            P("fs", "tp"),
            P("fs", "tp"),
            P("fs", "tp"),
            P("fs", "tp"),
            P(None, "tp"),
            P(None, "tp"),
        ),
        check_vma=False,
    )
```

profile of v0, /device:TPU:0, one launch (start us, length us, event | category | flops | bytes accessed | tf_op | source)
XLA Modules:
  0.0 486.5 jit_solution(8330795833223261178)
XLA Ops:
  7.2 0.0 copy-start
  7.2 0.0 all-gather.7.cloned.1.call-start
  7.2 0.7 all-gather.7.cloned.1.call-update
  7.9 0.0 all-gather.5.cloned.1.call-start
  8.0 0.7 all-gather.5.cloned.1.call-update
  8.7 0.0 copy-start.7
  8.7 0.0 reduce-scatter.5.cloned.1.call-start
  8.7 53.2 %all-gather.7.cloned.1.call-done = bf16[4096,256]{1,0:T(8,128)(2,1)} async-done(((bf16[512,256]{1,0:T(8,128)(2,1)}), bf16[4096,256]{1,0:T(8,128)(2,1)}) %all-gather.7.cloned.1.call-update) | async-done | bytes 2097168 | tf_op jit(solution)/shard_map/all_gather | solution.py:52
  62.0 0.0 copy-done
  62.0 2.3 fusion.8
  64.3 1.2 fusion.9
  65.5 0.0 reduce-scatter.5.cloned.1.call-update
  65.5 0.0 copy-start.4
  65.5 0.0 reduce-scatter.3.cloned.1.call-start
  65.6 46.2 %all-gather.5.cloned.1.call-done = bf16[4096,256]{1,0:T(8,128)(2,1)} async-done(((bf16[512,256]{1,0:T(8,128)(2,1)}), bf16[4096,256]{1,0:T(8,128)(2,1)}) %all-gather.5.cloned.1.call-update) | async-done | bytes 2097168 | tf_op jit(solution)/shard_map/all_gather | solution.py:47
  111.7 2.9 fusion.6
  114.7 0.0 copy-start.8
  114.7 0.0 copy-start.2
  114.7 2.2 fusion.7
  116.9 0.0 reduce-scatter.3.cloned.1.call-update
  116.9 0.0 all-gather.11.cloned.1.call-start
  117.0 59.9 %reduce-scatter.5.cloned.1.call-done = f32[32,512]{1,0:T(8,128)} async-done(((f32[256,512]{1,0:T(8,128)}), f32[32,512]{1,0:T(8,128)}) %reduce-scatter.5.cloned.1.call-update) | async-done | bytes 65552 | tf_op jit(solution)/shard_map/reduce_scatter | solution.py:59
  176.9 1.5 multiply_reduce_fusion
  178.4 63.9 %reduce-scatter.3.cloned.1.call-done = f32[32,512]{1,0:T(8,128)} async-done(((f32[256,512]{1,0:T(8,128)}), f32[32,512]{1,0:T(8,128)}) %reduce-scatter.3.cloned.1.call-update) | async-done | bytes 65552 | tf_op jit(solution)/shard_map/reduce_scatter | solution.py:58
  242.3 1.5 multiply_reduce_fusion.1
  245.1 0.0 copy-done.4
  245.1 1.3 copy.23
  246.4 39.9 %psum.7 = f32[]{:T(128)} all-reduce(f32[]{:T(128)S(6)} %add.24), channel_id=1, replica_groups=mesh['fs'=8,'tp'=4] {'fs','tp'}, use_global_device_ids=true, to_apply=%region_4.0 | all-reduce | flops 1 | bytes 8 | tf_op jit(solution)/shard_map/psum | solution.py:62
  287.0 1.5 multiply_convert_fusion
  288.5 30.7 %all_gather.21 = bf16[256,512]{1,0:T(8,128)(2,1)S(1)} all-gather(bf16[32,512]{1,0:T(8,128)(2,1)S(1)} %get-tuple-element.24), channel_id=1, replica_groups=mesh['fs'=8,'tp'=4] {'fs'}, dimensions={0}, use_global_device_ids=true | all-gather | bytes 294912 | tf_op jit(solution)/shard_map/all_gather | solution.py:68
  319.3 0.0 copy-done.2
  319.3 2.8 fusion.2
  322.1 0.0 all-gather.11.cloned.1.call-update
  322.1 0.0 all-gather.9.cloned.1.call-start
  322.1 2.6 copy.22
  324.7 0.0 copy-done.9
  324.7 1.5 multiply_convert_fusion.1
  326.3 32.0 %all_gather.20 = bf16[256,512]{1,0:T(8,128)(2,1)S(1)} all-gather(bf16[32,512]{1,0:T(8,128)(2,1)S(1)} %get-tuple-element.27), channel_id=1, replica_groups=mesh['fs'=8,'tp'=4] {'fs'}, dimensions={0}, use_global_device_ids=true | all-gather | bytes 294912 | tf_op jit(solution)/shard_map/all_gather | solution.py:67
  358.3 3.1 fusion.3
  361.4 0.0 all-gather.9.cloned.1.call-update
  361.4 2.6 copy.25
  364.0 1.3 copy.27
  365.3 2.6 copy.24
  367.9 1.3 copy.26
  369.2 28.7 %all-gather.11.cloned.1.call-done = bf16[4096,512]{0,1:T(8,128)(2,1)} async-done(((bf16[512,512]{0,1:T(8,128)(2,1)}), bf16[4096,512]{0,1:T(8,128)(2,1)}) %all-gather.11.cloned.1.call-update) | async-done | bytes 4194320 | tf_op jit(solution)/shard_map/all_gather | solution.py:76
  397.9 6.4 %copy.29 = bf16[4096,512]{1,0:T(8,128)(2,1)} copy(bf16[4096,512]{0,1:T(8,128)(2,1)} %all-gather.11.cloned.1.call-done) | data formatting | bytes 8388608
  404.3 68.9 %all-gather.9.cloned.1.call-done = bf16[4096,512]{0,1:T(8,128)(2,1)} async-done(((bf16[512,512]{0,1:T(8,128)(2,1)}), bf16[4096,512]{0,1:T(8,128)(2,1)}) %all-gather.9.cloned.1.call-update) | async-done | bytes 4194320 | tf_op jit(solution)/shard_map/all_gather | solution.py:75
  473.2 6.4 %copy.28 = bf16[4096,512]{1,0:T(8,128)(2,1)} copy(bf16[4096,512]{0,1:T(8,128)(2,1)} %all-gather.9.cloned.1.call-done) | data formatting | bytes 8388608
  (11 shorter events, 0.0 us)
Async XLA Ops:
  7.2 54.8 %copy-start = (bf16[256,4096]{1,0:T(8,128)(2,1)S(1)}, bf16[256,4096]{1,0:T(8,128)(2,1)}, u32[]{:S(2)}) copy-start(bf16[256,4096]{1,0:T(8,128)(2,1)} %param.14) | copy-start | bytes 6291460
  7.2 54.8 %all-gather.7.cloned.1.call-start = ((), (), s32[]{:S(2)}) async-start(), calls=%async_computation.4 | async-start | bytes 2359296 | tf_op jit(solution)/shard_map/all_gather | solution.py:52
  7.9 103.8 %all-gather.5.cloned.1.call-start = ((), (), s32[]{:S(2)}) async-start(), calls=%async_computation.2 | async-start | bytes 2359296 | tf_op jit(solution)/shard_map/all_gather | solution.py:47
  8.7 55.6 %copy-start.7 = (bf16[256,512]{1,0:T(8,128)(2,1)S(1)}, bf16[256,512]{1,0:T(8,128)(2,1)}, u32[]{:S(2)}) copy-start(bf16[256,512]{1,0:T(8,128)(2,1)} %param.15) | copy-start | bytes 786436
  8.7 168.2 %reduce-scatter.5.cloned.1.call-start = ((), (), s32[]{:S(2)}) async-start(), calls=%async_computation.5 | async-start | bytes 589824 | tf_op jit(solution)/shard_map/reduce_scatter | solution.py:59
  65.5 179.5 %copy-start.4 = (f32[512,512]{1,0:T(8,128)S(1)}, f32[512,512]{1,0:T(8,128)}, u32[]{:S(2)}) copy-start(f32[512,512]{1,0:T(8,128)} %param.19) | copy-start | bytes 3145732
  65.5 176.8 %reduce-scatter.3.cloned.1.call-start = ((), (), s32[]{:S(2)}) async-start(), calls=%async_computation.3 | async-start | bytes 589824 | tf_op jit(solution)/shard_map/reduce_scatter | solution.py:58
  114.7 172.3 %copy-start.8 = (f32[32,512]{1,0:T(8,128)S(1)}, f32[32,512]{1,0:T(8,128)}, u32[]{:S(2)}) copy-start(f32[32,512]{1,0:T(8,128)} %param.23) | copy-start | bytes 196612
  114.7 204.6 %copy-start.2 = (bf16[512,256]{1,0:T(8,128)(2,1)S(1)}, bf16[512,256]{1,0:T(8,128)(2,1)}, u32[]{:S(2)}) copy-start(bf16[512,256]{1,0:T(8,128)(2,1)} %param.17) | copy-start | bytes 786436
  116.9 281.0 %all-gather.11.cloned.1.call-start = ((), (), s32[]{:S(2)}) async-start(), calls=%async_computation.7 | async-start | bytes 4718592 | tf_op jit(solution)/shard_map/all_gather | solution.py:76
  176.8 110.2 %copy-start.6 = (f32[32,512]{1,0:T(8,128)S(1)}, f32[32,512]{1,0:T(8,128)}, u32[]{:S(2)}) copy-start(f32[32,512]{1,0:T(8,128)} %reduce-scatter.5.cloned.1.call-done) | copy-start | bytes 196612
  322.1 2.7 copy-start.5
  322.1 2.7 copy-start.9
  322.1 36.2 %copy-start.3 = (bf16[512,256]{1,0:T(8,128)(2,1)S(1)}, bf16[512,256]{1,0:T(8,128)(2,1)}, u32[]{:S(2)}) copy-start(bf16[512,256]{1,0:T(8,128)(2,1)} %param.16) | copy-start | bytes 786436
  322.1 151.1 %all-gather.9.cloned.1.call-start = ((), (), s32[]{:S(2)}) async-start(), calls=%async_computation.6 | async-start | bytes 4718592 | tf_op jit(solution)/shard_map/all_gather | solution.py:75
  365.3 2.6 copy-start.1
Sparse Core Ops, SparseCore 0:
  10.1 51.7 all-gather.6
  64.1 47.6 all-gather.4
  115.7 61.1 reduce-scatter.4
  180.6 61.6 reduce-scatter.2
  322.2 75.6 all-gather.10
  400.4 72.8 all-gather.8
where the time goes:
time: 487 us; the launch traced here: 486 us
  waiting for transfers between devices  322 us (66%)
  blocking collectives  103 us (21%)
  local copies, waits for them, and re-layouts  24.5 us (5%)
  between operations  16.2 us (3%)
  matrix products  14.6 us (3%)
  other arithmetic  6.02 us (1%)
    all_gather x1, waiting for transfers between devices, per_device(): lax.all_gather(query_weight.astype(jnp.bfloat16), 'fs', axis=0, tiled=True)  68.9 us
    reduce_scatter x1, waiting for transfers between devices, per_device(): lax.psum_scatter(query_part, 'fs', scatter_dimension=0, tiled=True)  63.9 us
    reduce_scatter x1, waiting for transfers between devices, per_device(): lax.psum_scatter(output_part, 'fs', scatter_dimension=0, tiled=True)  59.9 us
    all_gather x1, waiting for transfers between devices, per_device(): lax.all_gather(output_basis, 'fs', axis=0, tiled=True)  53.2 us
    all_gather x1, waiting for transfers between devices, per_device(): lax.all_gather(query_basis, 'fs', axis=0, tiled=True)  46.2 us
    psum x1, blocking collectives, per_device(): total_squares = lax.psum(local_squares, ('fs', 'tp'))  39.9 us
    all_gather x1, blocking collectives, per_device(): lax.all_gather(qdir, 'fs', axis=0, tiled=True)  32 us
    all_gather x1, blocking collectives, per_device(): lax.all_gather(odir, 'fs', axis=0, tiled=True)  30.7 us
  transfers between devices with their start and end apart: 6, of which 6 were waited for; matrix products, arithmetic and copies ran while one was open for 6% of the time, Pallas kernels for 0%

commit v1 on v0

--- a/solution.py
+++ b/solution.py
@@ -8,6 +8,13 @@
 beta_one = 0.8
 beta_two = 0.9
 rate = 0.1
+
+
+def all_by_exchange(block, mesh_axis, dim):
+    devices = lax.axis_size(mesh_axis)
+    shards = jnp.stack([block for _ in range(devices)])
+    shards = lax.all_to_all(shards, mesh_axis, split_axis=0, concat_axis=0)
+    return jnp.concatenate(shards, axis=dim)
 
 
 def moment_update(low, factor, first, second):
@@ -43,9 +50,7 @@
     output_second,
 ):
     query_coords = jnp.dot(
-        saved_input,
-        lax.all_gather(query_basis, "fs", axis=0, tiled=True),
-        preferred_element_type=jnp.float32,
+        saved_input, all_by_exchange(query_basis, "fs", 0), preferred_element_type=jnp.float32
     )
     output_coords = jnp.dot(
         layer_cotangent,

time: 487 us -> 467 us (0.959)
  waiting for transfers between devices: 322 us -> 293 us
  starting transfers between devices: 0.24 us -> 7.49 us
    all_gather x1 -> x0, waiting for transfers between devices: 46.2 us -> none  [per_device(): lax.all_gather(query_basis, 'fs', axis=0, tiled=True)]
    all_gather x1, waiting for transfers between devices: 68.9 us -> 28.5 us  [per_device(): lax.all_gather(query_weight.astype(jnp.bfloat16), 'fs', axis=0, tiled=True)]
    all_gather x1, waiting for transfers between devices: 28.7 us -> 68.3 us  [per_device(): lax.all_gather(output_weight.astype(jnp.bfloat16), 'fs', axis=0, tiled=True)]
    all_gather x1, waiting for transfers between devices: 53.2 us -> 75 us  [per_device(): lax.all_gather(output_basis, 'fs', axis=0, tiled=True)]
    all_to_all x0 -> x1, starting transfers between devices: none -> 7.28 us  [all_by_exchange(): shards = lax.all_to_all(shards, mesh_axis, split_axis=0, concat_axis=0)]
    unnamed x28 -> x30, local copies, waits for them, and re-layouts: 24.5 us -> 24.5 us
  transfers between devices with their start and end apart: 6 -> 6, of which waited for: 6 -> 5; matrix products, arithmetic and copies ran while one was open for 6% -> 7% of each run, Pallas kernels for 0% -> 0%
where the time goes in v1:
time: 467 us; the launch traced here: 466 us
  waiting for transfers between devices  293 us (63%)
  blocking collectives  103 us (22%)
  local copies, waits for them, and re-layouts  26.9 us (6%)
  between operations  15.9 us (3%)
  matrix products  13.7 us (3%)
  starting transfers between devices  7.49 us (2%)
  other arithmetic  6.02 us (1%)
    all_gather x1, waiting for transfers between devices, per_device(): lax.all_gather(output_basis, 'fs', axis=0, tiled=True)  75 us
    all_gather x1, waiting for transfers between devices, per_device(): lax.all_gather(output_weight.astype(jnp.bfloat16), 'fs', axis=0, tiled=True)  68.3 us
    reduce_scatter x1, waiting for transfers between devices, per_device(): lax.psum_scatter(query_part, 'fs', scatter_dimension=0, tiled=True)  64.2 us
    reduce_scatter x1, waiting for transfers between devices, per_device(): lax.psum_scatter(output_part, 'fs', scatter_dimension=0, tiled=True)  56.2 us
    psum x1, blocking collectives, per_device(): total_squares = lax.psum(local_squares, ('fs', 'tp'))  40 us
    all_gather x1, blocking collectives, per_device(): lax.all_gather(odir, 'fs', axis=0, tiled=True)  32.2 us
    all_gather x1, blocking collectives, per_device(): lax.all_gather(qdir, 'fs', axis=0, tiled=True)  30.7 us
    all_gather x1, waiting for transfers between devices, per_device(): lax.all_gather(query_weight.astype(jnp.bfloat16), 'fs', axis=0, tiled=True)  28.5 us
  transfers between devices with their start and end apart: 6, of which 5 were waited for; matrix products, arithmetic and copies ran while one was open for 7% of the time, Pallas kernels for 0%

profile of v1, /device:TPU:0, one launch (start us, length us, event | category | flops | bytes accessed | tf_op | source)
XLA Modules:
  0.0 466.0 jit_solution(12704365700582514130)
XLA Ops:
  7.2 0.0 copy-start
  7.2 0.0 all-gather.4.cloned.1.call-start
  7.2 0.7 all-gather.4.cloned.1.call-update
  7.9 2.4 stack.2
  10.3 7.3 %all-to-all-start = ((bf16[8,512,256]{2,1,0:T(8,128)(2,1)}), bf16[8,512,256]{2,1,0:T(8,128)(2,1)}, u32[]{:S(2)}, u32[]{:S(2)}) async-start(bf16[8,512,256]{2,1,0:T(8,128)(2,1)} %stack.2), calls=%async_computation | async-start | bytes 4194304 | tf_op jit(solution)/shard_map/all_to_all | solution.py:16
  17.6 0.0 reduce-scatter.5.cloned.1.call-start
  17.7 75.0 %all-gather.4.cloned.1.call-done = bf16[4096,256]{1,0:T(8,128)(2,1)} async-done(((bf16[512,256]{1,0:T(8,128)(2,1)}), bf16[4096,256]{1,0:T(8,128)(2,1)}) %all-gather.4.cloned.1.call-update) | async-done | bytes 2097168 | tf_op jit(solution)/shard_map/all_gather | solution.py:57
  92.7 0.0 copy-done
  92.7 2.3 fusion.8
  95.0 0.0 copy-done.7
  95.0 1.2 fusion.9
  96.2 0.0 reduce-scatter.5.cloned.1.call-update
  96.3 0.0 reduce-scatter.3.cloned.1.call-start
  96.3 0.0 all-to-all-done
  96.3 0.0 copy-start.8
  96.3 0.0 copy-start.4
  96.3 3.0 fusion.6
  99.4 0.0 copy-done.8
  99.4 0.0 copy-start.9
  99.4 0.0 copy-start.2
  99.4 1.2 fusion.7
  100.6 0.0 reduce-scatter.3.cloned.1.call-update
  100.6 0.0 all-gather.6.cloned.1.call-start
  100.7 56.2 %reduce-scatter.5.cloned.1.call-done = f32[32,512]{1,0:T(8,128)} async-done(((f32[256,512]{1,0:T(8,128)}), f32[32,512]{1,0:T(8,128)}) %reduce-scatter.5.cloned.1.call-update) | async-done | bytes 65552 | tf_op jit(solution)/shard_map/reduce_scatter | solution.py:64
  156.9 1.5 multiply_reduce_fusion
  158.4 64.2 %reduce-scatter.3.cloned.1.call-done = f32[32,512]{1,0:T(8,128)} async-done(((f32[256,512]{1,0:T(8,128)}), f32[32,512]{1,0:T(8,128)}) %reduce-scatter.3.cloned.1.call-update) | async-done | bytes 65552 | tf_op jit(solution)/shard_map/reduce_scatter | solution.py:63
  222.6 1.5 multiply_reduce_fusion.1
  225.4 1.3 copy.22
  226.7 40.0 %psum.7 = f32[]{:T(128)} all-reduce(f32[]{:T(128)S(6)} %add.24), channel_id=1, replica_groups=mesh['fs'=8,'tp'=4] {'fs','tp'}, use_global_device_ids=true, to_apply=%region_4.0 | all-reduce | flops 1 | bytes 8 | tf_op jit(solution)/shard_map/psum | solution.py:67
  267.4 1.5 multiply_convert_fusion.1
  268.9 30.7 %all_gather.16 = bf16[256,512]{1,0:T(8,128)(2,1)S(1)} all-gather(bf16[32,512]{1,0:T(8,128)(2,1)S(1)} %get-tuple-element.27), channel_id=1, replica_groups=mesh['fs'=8,'tp'=4] {'fs'}, dimensions={0}, use_global_device_ids=true | all-gather | bytes 294912 | tf_op jit(solution)/shard_map/all_gather | solution.py:72
  299.7 2.8 fusion.3
  302.5 0.0 all-gather.6.cloned.1.call-update
  302.5 0.0 all-gather.8.cloned.1.call-start
  302.6 2.6 copy.23
  305.1 0.0 copy-done.10
  305.1 1.5 multiply_convert_fusion
  306.7 32.2 %all_gather.17 = bf16[256,512]{1,0:T(8,128)(2,1)S(1)} all-gather(bf16[32,512]{1,0:T(8,128)(2,1)S(1)} %get-tuple-element.24), channel_id=1, replica_groups=mesh['fs'=8,'tp'=4] {'fs'}, dimensions={0}, use_global_device_ids=true | all-gather | bytes 294912 | tf_op jit(solution)/shard_map/all_gather | solution.py:73
  338.8 3.2 fusion.2
  342.0 0.0 all-gather.8.cloned.1.call-update
  342.0 2.6 copy.24
  344.6 1.3 copy.26
  345.9 2.6 copy.25
  348.5 1.3 copy.27
  349.8 28.5 %all-gather.6.cloned.1.call-done = bf16[4096,512]{0,1:T(8,128)(2,1)} async-done(((bf16[512,512]{0,1:T(8,128)(2,1)}), bf16[4096,512]{0,1:T(8,128)(2,1)}) %all-gather.6.cloned.1.call-update) | async-done | bytes 4194320 | tf_op jit(solution)/shard_map/all_gather | solution.py:80
  378.3 6.4 %copy.28 = bf16[4096,512]{1,0:T(8,128)(2,1)} copy(bf16[4096,512]{0,1:T(8,128)(2,1)} %all-gather.6.cloned.1.call-done) | data formatting | bytes 8388608
  384.7 68.3 %all-gather.8.cloned.1.call-done = bf16[4096,512]{0,1:T(8,128)(2,1)} async-done(((bf16[512,512]{0,1:T(8,128)(2,1)}), bf16[4096,512]{0,1:T(8,128)(2,1)}) %all-gather.8.cloned.1.call-update) | async-done | bytes 4194320 | tf_op jit(solution)/shard_map/all_gather | solution.py:81
  453.1 6.4 %copy.29 = bf16[4096,512]{1,0:T(8,128)(2,1)} copy(bf16[4096,512]{0,1:T(8,128)(2,1)} %all-gather.8.cloned.1.call-done) | data formatting | bytes 8388608
  (13 shorter events, 0.0 us)
Async XLA Ops:
  7.2 85.5 %copy-start = (bf16[256,4096]{1,0:T(8,128)(2,1)S(1)}, bf16[256,4096]{1,0:T(8,128)(2,1)}, u32[]{:S(2)}) copy-start(bf16[256,4096]{1,0:T(8,128)(2,1)} %param.14) | copy-start | bytes 6291460
  7.2 85.5 %all-gather.4.cloned.1.call-start = ((), (), s32[]{:S(2)}) async-start(), calls=%async_computation.4 | async-start | bytes 2359296 | tf_op jit(solution)/shard_map/all_gather | solution.py:57
  10.3 86.0 %all-to-all-start = ((bf16[8,512,256]{2,1,0:T(8,128)(2,1)}), bf16[8,512,256]{2,1,0:T(8,128)(2,1)}, u32[]{:S(2)}, u32[]{:S(2)}) async-start(bf16[8,512,256]{2,1,0:T(8,128)(2,1)} %stack.2), calls=%async_computation | async-start | bytes 4194304 | tf_op jit(solution)/shard_map/all_to_all | solution.py:16
  17.6 77.4 %copy-start.7 = (bf16[256,512]{1,0:T(8,128)(2,1)S(1)}, bf16[256,512]{1,0:T(8,128)(2,1)}, u32[]{:S(2)}) copy-start(bf16[256,512]{1,0:T(8,128)(2,1)} %param.15) | copy-start | bytes 786436
  17.6 139.3 %reduce-scatter.5.cloned.1.call-start = ((), (), s32[]{:S(2)}) async-start(), calls=%async_computation.5 | async-start | bytes 589824 | tf_op jit(solution)/shard_map/reduce_scatter | solution.py:64
  96.3 126.3 %reduce-scatter.3.cloned.1.call-start = ((), (), s32[]{:S(2)}) async-start(), calls=%async_computation.3 | async-start | bytes 589824 | tf_op jit(solution)/shard_map/reduce_scatter | solution.py:63
  96.3 3.1 copy-start.8
  96.3 129.1 %copy-start.4 = (f32[512,512]{1,0:T(8,128)S(1)}, f32[512,512]{1,0:T(8,128)}, u32[]{:S(2)}) copy-start(f32[512,512]{1,0:T(8,128)} %param.18) | copy-start | bytes 3145732
  99.4 168.0 %copy-start.9 = (f32[32,512]{1,0:T(8,128)S(1)}, f32[32,512]{1,0:T(8,128)}, u32[]{:S(2)}) copy-start(f32[32,512]{1,0:T(8,128)} %param.21) | copy-start | bytes 196612
  99.4 200.3 %copy-start.2 = (bf16[512,256]{1,0:T(8,128)(2,1)S(1)}, bf16[512,256]{1,0:T(8,128)(2,1)}, u32[]{:S(2)}) copy-start(bf16[512,256]{1,0:T(8,128)(2,1)} %param.16) | copy-start | bytes 786436
  100.6 277.7 %all-gather.6.cloned.1.call-start = ((), (), s32[]{:S(2)}) async-start(), calls=%async_computation.6 | async-start | bytes 4718592 | tf_op jit(solution)/shard_map/all_gather | solution.py:80
  222.6 44.8 %copy-start.6 = (f32[32,512]{1,0:T(8,128)S(1)}, f32[32,512]{1,0:T(8,128)}, u32[]{:S(2)}) copy-start(f32[32,512]{1,0:T(8,128)} %reduce-scatter.3.cloned.1.call-done) | copy-start | bytes 196612
  302.5 2.7 copy-start.5
  302.5 2.7 copy-start.10
  302.5 36.4 %copy-start.3 = (bf16[512,256]{1,0:T(8,128)(2,1)S(1)}, bf16[512,256]{1,0:T(8,128)(2,1)}, u32[]{:S(2)}) copy-start(bf16[512,256]{1,0:T(8,128)(2,1)} %param.17) | copy-start | bytes 786436
  302.5 150.6 %all-gather.8.cloned.1.call-start = ((), (), s32[]{:S(2)}) async-start(), calls=%async_computation.7 | async-start | bytes 4718592 | tf_op jit(solution)/shard_map/all_gather | solution.py:81
  345.9 2.6 copy-start.1
Sparse Core Ops, SparseCore 0:
  10.1 82.5 all-gather.3
  96.6 60.2 reduce-scatter.4
  160.8 61.6 reduce-scatter.2
  302.6 75.6 all-gather.5
  380.2 72.8 all-gather.7
